TPU v7x, 32 devices: a whole 2x2x4 slice. The times are simulated.
32 devices in a mesh: sp: 16 (over z, y, x), tp: 2 (over core).
Axes of the slice: x: 2, y: 2, z: 4, core: 2. Of those that a mesh axis runs over, the one named last changes fastest.
Arguments:
- acceptor_signal: bfloat16 [2048, 1024], P('sp', 'tp'), may hold values from -6 to 6
- address_entries: bfloat16 [2048, 1024], P('sp', 'tp'), may hold values from -6 to 6
- payload_entries: bfloat16 [2048, 1024], P('sp', 'tp'), may hold values from -6 to 6
- fading_logits: float32 [2048, 1024], P('sp', 'tp'), may hold values from -12 to -2
- learning_rate_logits: float32 [2048, 1024], P('sp', 'tp'), may hold values from -10 to 4
- exit_switch_entries: bfloat16 [2048, 1024], P('sp', 'tp'), may hold values from -6 to 6
- extra_reward_weights: float32 [1024], P('tp'), may hold values from -0.3 to 0.3
- subspace_rescale_weights: float32 [1024], P('tp'), may hold values from 0.1 to 1.9
- timemix_exit_weights: bfloat16 [1024, 2048], P('tp'), may hold values from -0.1875 to 0.1875
- skip_stream_arriving: bfloat16 [2048, 2048], P(('sp', 'tp')), may hold values from -6 to 6
- pointwise_block_scaling: float32 [2048], replicated, may hold values from 0.1 to 1.9
- switch_projection: bfloat16 [2048, 5632], P('sp', 'tp'), may hold values from -0.125 to 0.125
- widening_projection: bfloat16 [2048, 5632], P('sp', 'tp'), may hold values from -0.125 to 0.125
- switch_filter_coefficients: float32 [3, 5632], P(None, 'tp'), may hold values from -3.5 to 3.5
- narrowing_projection: bfloat16 [5632, 2048], P('tp', 'sp'), may hold values from -0.078125 to 0.078125
Outputs:
- layer_out: bfloat16 [2048, 2048], P(('sp', 'tp'))
All inputs are finite; a program needn't handle non-finite values.
Results may differ from a plain program's by a relative error of at most 0.019.
Values may be sent and summed in bfloat16 or wider, within the bound.
A program may use at most 128 MiB of HBM per device.

v0:
```python
import jax
import jax.numpy as jnp
from jax import lax
from jax.sharding import PartitionSpec as P

SUBSPACE_WIDTH = 64
SPAN = 16
group_eps = 0.00064
norm_eps = 1e-06
highest = lax.Precision.HIGHEST


def carried_in(shard, axis, join, neutral):
    place = lax.axis_index(axis)
    gathered = jax.tree.map(
        lambda a, kind: lax.all_gather(a.astype(kind), axis), shard, (jnp.bfloat16, jnp.bfloat16)
    )
    state = jax.tree.map(lambda a, e: jnp.zeros_like(a) + jnp.asarray(e, a.dtype), shard, neutral)

    def one(lap, state):
        return join(
            state,
            jax.tree.map(
                lambda a, own: lax.dynamic_index_in_dim(a, lap, 0, False).astype(own.dtype),
                gathered,
                shard,
            ),
        )

    return lax.fori_loop(0, place, one, state)


def shifted(block, axis, distance):
    devices = range(lax.axis_size(axis))
    route = [(i - distance, i) for i in devices if i - distance in devices]
    return lax.ppermute(block, axis, route)


def by_heads(array):
    return array.astype(jnp.float32).reshape(array.shape[0], -1, SUBSPACE_WIDTH)


def mechanism_inputs(
    acceptor_signal, address_entries, payload_entries, fading_logits, learning_rate_logits
):
    acceptor_entries = by_heads(acceptor_signal)
    address_mapped = by_heads(address_entries)
    payload_mapped = by_heads(payload_entries)
    log_rate = -jax.nn.softplus(-fading_logits) - 0.5
    fading = by_heads(jnp.exp(-jnp.exp(log_rate)))
    erase_rate = by_heads(jax.nn.sigmoid(learning_rate_logits))
    length = jnp.sqrt(jnp.sum(address_mapped * address_mapped, axis=-1, keepdims=True))
    unit_key = address_mapped / jnp.maximum(length, 1.0)
    return (
        acceptor_entries,
        address_mapped,
        payload_mapped,
        fading,
        -unit_key,
        unit_key * erase_rate,
    )


def subspace_outcomes(
    acceptor_entries,
    address_mapped,
    payload_mapped,
    closing_memory,
    subspace_rescale_weights,
    extra_reward_weights,
    exit_switch_entries,
):
    centred = closing_memory - jnp.mean(closing_memory, axis=-1, keepdims=True)
    rescaled_arguments = centred * lax.rsqrt(
        jnp.mean(centred * centred, axis=-1, keepdims=True) + group_eps
    )
    scaling_fetch = subspace_rescale_weights.reshape(-1, SUBSPACE_WIDTH)
    extra_reward_fetch = extra_reward_weights.reshape(-1, SUBSPACE_WIDTH)
    present_extra_reward = (
        jnp.sum(acceptor_entries * address_mapped * extra_reward_fetch, axis=-1, keepdims=True)
        * payload_mapped
    )
    timemix_product = rescaled_arguments * scaling_fetch + present_extra_reward
    timemix_product = timemix_product.reshape(
        timemix_product.shape[0], -1
    ) * exit_switch_entries.astype(jnp.float32)
    return timemix_product.astype(jnp.bfloat16)


def compose(earlier, latter):
    mapping = jnp.einsum("...ij,...jk->...ik", earlier[0], latter[0], precision=highest)
    state = jnp.einsum("...ij,...jk->...ik", earlier[1], latter[0], precision=highest) + latter[1]
    return (mapping, state)


def span_step(carried, sublevel_arguments):
    state, mapping = carried
    acceptor_entries, address_mapped, payload_mapped, fading, erase_dir, erase_amt = (
        sublevel_arguments
    )
    along = jnp.einsum("bhij,bhj->bhi", state, erase_dir, precision=highest)
    map_along = jnp.einsum("bhij,bhj->bhi", mapping, erase_dir, precision=highest)
    state = (
        state * fading[:, :, None, :]
        + along[..., None] * erase_amt[:, :, None, :]
        + payload_mapped[..., None] * address_mapped[:, :, None, :]
    )
    mapping = mapping * fading[:, :, None, :] + map_along[..., None] * erase_amt[:, :, None, :]
    local_out = jnp.einsum("bhij,bhj->bhi", state, acceptor_entries, precision=highest)
    probe = jnp.einsum("bhij,bhj->bhi", mapping, acceptor_entries, precision=highest)
    return ((state, mapping), (local_out, probe))


def recurrence(sublevel_arguments):
    token_count, head_count = (sublevel_arguments[0].shape[0], sublevel_arguments[0].shape[1])
    blocks = token_count // SPAN

    def arrange(member):
        return jnp.moveaxis(member.reshape(blocks, SPAN, head_count, SUBSPACE_WIDTH), 1, 0)

    arranged = tuple((arrange(member) for member in sublevel_arguments))
    unit_map = jnp.eye(SUBSPACE_WIDTH, dtype=jnp.float32)
    zero_state = jnp.zeros((blocks, head_count, SUBSPACE_WIDTH, SUBSPACE_WIDTH), jnp.float32)
    start_maps = jnp.broadcast_to(unit_map, zero_state.shape)
    (block_states, block_maps), (local_out, probe) = lax.scan(
        span_step, (zero_state, start_maps), arranged
    )
    cum_maps, cum_states = lax.associative_scan(compose, (block_maps, block_states))
    head_unit = jnp.broadcast_to(unit_map, (head_count, SUBSPACE_WIDTH, SUBSPACE_WIDTH))
    head_zero = jnp.zeros((head_count, SUBSPACE_WIDTH, SUBSPACE_WIDTH), jnp.float32)
    _, incoming = carried_in((cum_maps[-1], cum_states[-1]), "sp", compose, (head_unit, head_zero))
    prior_maps = jnp.concatenate([head_unit[None], cum_maps[:-1]], axis=0)
    prior_states = jnp.concatenate([head_zero[None], cum_states[:-1]], axis=0)
    entry = jnp.einsum("hij,bhjk->bhik", incoming, prior_maps, precision=highest) + prior_states
    closing_memory = local_out + jnp.einsum("bhij,tbhj->tbhi", entry, probe, precision=highest)
    return jnp.moveaxis(closing_memory, 0, 1).reshape(token_count, head_count, SUBSPACE_WIDTH)


def body(
    acceptor_signal,
    address_entries,
    payload_entries,
    fading_logits,
    learning_rate_logits,
    exit_switch_entries,
    extra_reward_weights,
    subspace_rescale_weights,
    timemix_exit_weights,
    skip_stream_arriving,
    pointwise_block_scaling,
    switch_projection,
    widening_projection,
    switch_filter_coefficients,
    narrowing_projection,
):
    gate_full, up_full, down_full = (
        lax.all_gather(switch_projection, "sp", axis=0, tiled=True),
        lax.all_gather(widening_projection, "sp", axis=0, tiled=True),
        lax.all_gather(narrowing_projection, "sp", axis=1, tiled=True),
    )
    sublevel_arguments = mechanism_inputs(
        acceptor_signal, address_entries, payload_entries, fading_logits, learning_rate_logits
    )
    closing_memory = recurrence(sublevel_arguments)
    timemix_product = subspace_outcomes(
        sublevel_arguments[0],
        sublevel_arguments[1],
        sublevel_arguments[2],
        closing_memory,
        subspace_rescale_weights,
        extra_reward_weights,
        exit_switch_entries,
    )
    token_count = timemix_product.shape[0]
    picked = timemix_product
    attended = lax.psum_scatter(
        jnp.dot(picked, timemix_exit_weights, preferred_element_type=jnp.float32).astype(
            jnp.bfloat16
        ),
        "tp",
        scatter_dimension=0,
        tiled=True,
    ).astype(jnp.float32)
    hidden_res = skip_stream_arriving.astype(jnp.float32) + attended
    rescaled_arguments = (
        hidden_res
        * lax.rsqrt(jnp.mean(hidden_res * hidden_res, axis=-1, keepdims=True) + norm_eps)
        * pointwise_block_scaling
    )
    rescaled_arguments = rescaled_arguments.astype(jnp.bfloat16)
    all_rows = lax.all_gather(rescaled_arguments, "tp", axis=0, tiled=True)
    gate_acc = jnp.dot(all_rows, gate_full, preferred_element_type=jnp.float32)
    up_acc = jnp.dot(all_rows, up_full, preferred_element_type=jnp.float32)
    gate_pre = gate_acc.astype(jnp.bfloat16)
    up_part = up_acc.astype(jnp.bfloat16)
    taps = switch_filter_coefficients.shape[0]
    tail_rows = shifted(gate_pre[token_count - taps + 1 :], "sp", 1)
    extended = jnp.concatenate([tail_rows, gate_pre], axis=0).astype(jnp.float32)
    conv_out = jnp.zeros(gate_pre.shape, jnp.float32)
    for tap in range(taps):
        conv_out = conv_out + switch_filter_coefficients[tap] * extended[tap : tap + token_count]
    hidden = (jax.nn.silu(conv_out) * up_part.astype(jnp.float32)).astype(jnp.bfloat16)
    picked = hidden
    projected = lax.psum_scatter(
        jnp.dot(picked, down_full, preferred_element_type=jnp.float32).astype(jnp.bfloat16),
        "tp",
        scatter_dimension=0,
        tiled=True,
    ).astype(jnp.float32)
    return (hidden_res + projected).astype(jnp.bfloat16)


def solution(mesh):
    return jax.shard_map(
        body,
        mesh=mesh,
        in_specs=(
            P("sp", "tp"),
            P("sp", "tp"),
            P("sp", "tp"),
            P("sp", "tp"),
            P("sp", "tp"),
            P("sp", "tp"),
            P("tp"),
            P("tp"),
            P("tp", None),
            P(("sp", "tp"), None),
            P(),
            P("sp", "tp"),
            P("sp", "tp"),
            P(None, "tp"),
            P("tp", "sp"),
        ),
        out_specs=P(("sp", "tp"), None),
        check_vma=False,
    )
```

profile of v0, /device:TPU:0, one launch (start us, length us, event | category | flops | bytes accessed | tf_op | source)
XLA Modules:
  0.0 1192.7 jit_solution(1004884859613980477)
XLA Ops:
  23.3 418.0 %while.30 = (s32[]{:T(128)}, f32[8,8,64,64]{3,2,1,0:T(8,128)}, f32[8,8,64,64]{3,2,1,0:T(8,128)}, f32[16,8,8,64]{3,0,2,1:T(8,128)}, f32[16,8,8,64]{3,0,2,1:T(8,12...) while((s32[]{:T(128)}, f32[8,8,64,64]{3,2,1,0:T(8,128)}, ...), condition=%wide.region_2.3_spmd.clone, body=%wide.region_1.2_spmd.clone.sunk | while | flops 15204355 | bytes 25657612 | solution.py:125
  48.5 5.1 fusion.113
  74.8 5.1 fusion.113
  101.0 5.1 fusion.113
  127.2 5.1 fusion.113
  153.4 5.1 fusion.113
  452.4 9.2 pad.48
  463.5 9.2 pad.47
  478.5 16.6 %pad.50 = f32[8,8,64,64]{3,2,1,0:T(8,128)} pad(f32[4,8,64,64]{3,2,1,0:T(8,128)} %copy-done.6, f32[]{:T(128)} %constant.54.clone.1), padding=1_0_1x0_0_0x0_0_0x0_0_0 | pad | bytes 1572868 | tf_op jit(solution)/shard_map/pad | solution.py:128
  497.4 16.7 %pad.49 = f32[8,8,64,64]{3,2,1,0:T(8,128)} pad(f32[4,8,64,64]{3,2,1,0:T(8,128)} %pad_maximum_fusion.1, f32[]{:T(128)} %constant.54.clone.1), padding=0_1_1x0_0_0x0_0_0x0_0_0 | pad | bytes 1572868 | tf_op jit(solution)/shard_map/pad | solution.py:128
  518.8 5.9 pad.41
  525.8 5.9 pad.42
  533.4 11.1 pad.112
  546.2 16.6 %pad.67 = f32[7,8,64,64]{3,2,1,0:T(8,128)} pad(f32[4,8,64,64]{3,2,1,0:T(8,128)} %pad_maximum_fusion.1, f32[]{:T(128)} %constant.54.clone.1), padding=0_0_1x0_0_0x0_0_0x0_0_0 | pad | bytes 1441796 | tf_op jit(solution)/shard_map/slice | solution.py:133
  563.8 11.2 pad.44
  577.1 11.2 pad.43
  594.9 46.1 %all-gather.6.cloned.1.call-done = bf16[16,8,64,64]{3,2,1,0:T(8,128)(2,1)} async-done(((bf16[1,8,64,64]{3,2,1,0:T(8,128)(2,1)}), bf16[16,8,64,64]{3,2,1,0:T(8,128)(2,1)}) %all-gather.6.cloned.1.call-update) | async-done | bytes 1048592 | tf_op jit(solution)/shard_map/all_gather | solution.py:16
  654.4 39.6 %reduce-scatter.3.cloned.1.call-done = bf16[64,2048]{1,0:T(8,128)(2,1)} async-done(((bf16[128,2048]{1,0:T(8,128)(2,1)}), bf16[64,2048]{1,0:T(8,128)(2,1)}) %reduce-scatter.3.cloned.1.call-update) | async-done | bytes 262160 | tf_op jit(solution)/shard_map/reduce_scatter | solution.py:176
  698.4 140.8 %all-gather.10.cloned.1.call-done = bf16[2048,2816]{1,0:T(8,128)(2,1)} async-done(((bf16[128,2816]{1,0:T(8,128)(2,1)}), bf16[2048,2816]{1,0:T(8,128)(2,1)}) %all-gather.10.cloned.1.call-update) | async-done | bytes 11534352 | tf_op jit(solution)/shard_map/all_gather | solution.py:157
  839.1 6.0 convolution_convert_fusion.1
  851.0 130.4 %all-gather.12.cloned.1.call-done = bf16[2048,2816]{1,0:T(8,128)(2,1)} async-done(((bf16[128,2816]{1,0:T(8,128)(2,1)}), bf16[2048,2816]{1,0:T(8,128)(2,1)}) %all-gather.12.cloned.1.call-update) | async-done | bytes 11534352 | tf_op jit(solution)/shard_map/all_gather | solution.py:158
  981.4 182.8 %all-gather.14.cloned.1.call-done = bf16[2816,2048]{1,0:T(8,128)(2,1)} async-done(((bf16[2816,128]{1,0:T(8,128)(2,1)}), bf16[2816,2048]{1,0:T(8,128)(2,1)}) %all-gather.14.cloned.1.call-update) | async-done | bytes 11534352 | tf_op jit(solution)/shard_map/all_gather | solution.py:159
  1164.2 13.6 %convolution_convert_fusion.2 = bf16[128,2048]{1,0:T(8,128)(2,1)} fusion(bf16[2816,2048]{1,0:T(8,128)(2,1)} %all-gather.14.cloned.1.call-done, bf16[128,2048]{1,0:T(8,128)(2,1)S(1)} %all_gather.22, bf16[2048,2816]{1,0:T(8,128)(2,1)} %all-gather.12.cloned.1.call-done, f32[130,2816]{1,0:T(8,128)} %maximum_convert_fusion, f32[2816]{0:T(1024)S(1)} %get-tuple-element.188, ...), kind=kOutput, calls=%fused_computation.27 | convolution fusion | flops 2957737984 | bytes 28476416 | tf_op jit(solution)/shard_map/dot_general | solution.py:205
  1177.8 6.3 reduce-scatter.5.cloned.1.call-done
  (426 shorter events, 473.3 us)
Async XLA Ops:
  6.5 643.8 %copy-start = (bf16[512,2048]{1,0:T(8,128)(2,1)S(1)}, bf16[512,2048]{1,0:T(8,128)(2,1)}, u32[]{:S(2)}) copy-start(bf16[512,2048]{1,0:T(8,128)(2,1)} %param.27) | copy-start | bytes 6291460
  6.5 588.4 %all-gather.8.cloned.1.call-start = ((), (), s32[]{:S(2)}) async-start(), calls=%async_computation.3 | async-start | bytes 2228224 | tf_op jit(solution)/shard_map/all_gather | solution.py:16
  7.9 13.7 %copy-start.21 = (f32[64,64]{1,0:T(8,128)}, f32[64,64]{1,0:T(8,128)S(1)}, u32[]{:S(2)}) copy-start(f32[64,64]{1,0:T(8,128)S(1)} %fusion.61) | copy-start | bytes 49156
  48.5 10.0 copy-start.4
  74.8 10.0 copy-start.4
  101.0 10.0 copy-start.4
  127.2 10.0 copy-start.4
  153.4 10.0 copy-start.4
  179.6 10.0 copy-start.4
  450.7 10.9 slice-start
  478.5 16.6 %copy-start.17 = (f32[1,8,64,64]{3,2,1,0:T(8,128)S(1)}, f32[1,8,64,64]{3,2,1,0:T(8,128)}, u32[]{:S(2)}) copy-start(f32[1,8,64,64]{3,2,1,0:T(8,128)} %slice.129) | copy-start | bytes 393220
  515.8 125.2 %all-gather.6.cloned.1.call-start = ((), (), s32[]{:S(2)}) async-start(), calls=%async_computation.2 | async-start | bytes 2228224 | tf_op jit(solution)/shard_map/all_gather | solution.py:16
  546.1 147.8 %reduce-scatter.3.cloned.1.call-start = ((), (), s32[]{:S(2)}) async-start(), calls=%async_computation.4 | async-start | bytes 786432 | tf_op jit(solution)/shard_map/reduce_scatter | solution.py:176
  577.1 11.3 copy-start.26
  577.1 11.3 copy-start.16
  652.6 41.4 %copy-start.12 = (bf16[64,2048]{1,0:T(8,128)(2,1)S(1)}, bf16[64,2048]{1,0:T(8,128)(2,1)}, u32[]{:S(2)}) copy-start(bf16[64,2048]{1,0:T(8,128)(2,1)} %param.28) | copy-start | bytes 786436
  652.6 42.6 %copy-start.24 = (f32[2048]{0:T(1024)S(1)}, f32[2048]{0:T(1024)}, u32[]{:S(2)}) copy-start(f32[2048]{0:T(1024)} %param.29) | copy-start | bytes 24580
  652.6 186.6 %all-gather.10.cloned.1.call-start = ((), (), s32[]{:S(2)}) async-start(), calls=%async_computation.5 | async-start | bytes 12255232 | tf_op jit(solution)/shard_map/all_gather | solution.py:157
  653.2 328.2 %all-gather.12.cloned.1.call-start = ((), (), s32[]{:S(2)}) async-start(), calls=%async_computation.6 | async-start | bytes 12255232 | tf_op jit(solution)/shard_map/all_gather | solution.py:158
  653.7 510.5 %all-gather.14.cloned.1.call-start = ((), (), s32[]{:S(2)}) async-start(), calls=%async_computation.7 | async-start | bytes 12255232 | tf_op jit(solution)/shard_map/all_gather | solution.py:159
  654.3 529.8 %reduce-scatter.5.cloned.1.call-start = ((), (), s32[]{:S(2)}) async-start(), calls=%async_computation.8 | async-start | bytes 786432 | tf_op jit(solution)/shard_map/reduce_scatter | solution.py:204
  698.4 150.2 %copy-start.23 = (f32[3,2816]{1,0:T(4,128)S(1)}, f32[3,2816]{1,0:T(4,128)}, u32[]{:S(2)}) copy-start(f32[3,2816]{1,0:T(4,128)} %param.32) | copy-start | bytes 101380
  845.1 4.6 collective-permute-start
  1164.2 19.9 %copy-start.13 = (bf16[64,2048]{1,0:T(8,128)(2,1)S(1)}, bf16[64,2048]{1,0:T(8,128)(2,1)}, u32[]{:S(2)}) copy-start(bf16[64,2048]{1,0:T(8,128)(2,1)} %reduce-scatter.3.cloned.1.call-done) | copy-start | bytes 786436
  (72 other events, 321.6 us)
Sparse Core Ops, SparseCore 0:
  515.9 63.0 all-gather.7
  581.9 59.1 all-gather.5
  652.7 41.2 reduce-scatter.2
  696.6 142.5 all-gather.9
  841.7 139.5 all-gather.11
  983.9 180.2 all-gather.13
  1178.0 6.0 reduce-scatter.4
where the time goes:
time: 1210 us; the launch traced here: 1190 us
  waiting for transfers between devices  549 us (45%)
  matrix products  311 us (26%)
  local copies, waits for them, and re-layouts  248 us (20%)
  other arithmetic  64.1 us (5%)
  between operations  14.1 us (1%)
    all_gather x1, waiting for transfers between devices, body(): lax.all_gather(narrowing_projection, 'sp', axis=1, tiled=True)  183 us
    all_gather x1, waiting for transfers between devices, body(): lax.all_gather(switch_projection, 'sp', axis=0, tiled=True)  141 us
    all_gather x1, waiting for transfers between devices, body(): lax.all_gather(widening_projection, 'sp', axis=0, tiled=True)  130 us
    pad x8, local copies, waits for them, and re-layouts, recurrence(): lax.associative_scan(compose, (block_maps, block_states))  86 us
    dot_general x16, matrix products, span_step(): along = jnp.einsum('bhij,bhj->bhi', state, erase_dir, precision=highest)  79.9 us
    dot_general x16, matrix products, span_step(): jnp.einsum('bhij,bhj->bhi', state, acceptor_entries, precision=highest)  79 us
    dynamic_update_slice x32, local copies, waits for them, and re-layouts, recurrence(): lax.scan(span_step, (zero_state, start_maps), arranged)  57 us
    dot_general x16, matrix products, span_step(): jnp.einsum('bhij,bhj->bhi', mapping, erase_dir, precision=highest)  53.9 us
  transfers between devices with their start and end apart: 8, of which 7 were waited for; matrix products, arithmetic and copies ran while one was open for 7% of the time, Pallas kernels for 0%

commit v1 on v0

--- a/solution.py
+++ b/solution.py
@@ -8,6 +8,28 @@
 group_eps = 0.00064
 norm_eps = 1e-06
 highest = lax.Precision.HIGHEST
+
+
+def joined_along(blocks, dim):
+    dims = list(blocks.shape[1:])
+    dims[dim] *= blocks.shape[0]
+    return jnp.moveaxis(blocks, 0, dim).reshape(dims)
+
+
+def ring_gather(x, axis, dim):
+    size = lax.axis_size(axis)
+    pairs = [(i, (i + 1) % size) for i in range(size)]
+    back = [(b, a) for a, b in pairs]
+    lower, upper = ([], [])
+    for step in range(size - 1):
+        if step % 2 == 0:
+            lower.append(lax.ppermute(lower[-1] if lower else x, axis, pairs))
+        else:
+            upper.append(lax.ppermute(upper[-1] if upper else x, axis, back))
+    parts = jnp.stack([*lower[::-1], x, *upper])
+    shift = lax.axis_index(axis) - len(lower)
+    parts = parts[(jnp.arange(size) - shift) % size]
+    return joined_along(parts, dim)
 
 
 def carried_in(shard, axis, join, neutral):
@@ -156,7 +178,7 @@
     gate_full, up_full, down_full = (
         lax.all_gather(switch_projection, "sp", axis=0, tiled=True),
         lax.all_gather(widening_projection, "sp", axis=0, tiled=True),
-        lax.all_gather(narrowing_projection, "sp", axis=1, tiled=True),
+        ring_gather(narrowing_projection, "sp", 1),
     )
     sublevel_arguments = mechanism_inputs(
         acceptor_signal, address_entries, payload_entries, fading_logits, learning_rate_logits

time: 1210 us -> 1170 us (0.967)
  waiting for transfers between devices: 549 us -> 319 us
  starting transfers between devices: 3.68 us -> 138 us
  local copies, waits for them, and re-layouts: 248 us -> 297 us
    all_gather x1 -> x0, waiting for transfers between devices: 183 us -> none  [body(): lax.all_gather(narrowing_projection, 'sp', axis=1, tiled=True)]
    ppermute x0 -> x15, waiting for transfers between devices: none -> 178 us  [the longest x8 106 us: ring_gather(): lower.append(lax.ppermute(lower[-1] if lower else x, axis, pairs))]
    all_gather x1, waiting for transfers between devices: 141 us -> 0.01 us  [body(): lax.all_gather(switch_projection, 'sp', axis=0, tiled=True)]
    ppermute x0 -> x15, starting transfers between devices: none -> 136 us  [the longest x7 128 us: ring_gather(): upper.append(lax.ppermute(upper[-1] if upper else x, axis, back))]
    all_gather x1, waiting for transfers between devices: 130 us -> 87.5 us  [body(): lax.all_gather(widening_projection, 'sp', axis=0, tiled=True)]
    reduce_scatter x1, waiting for transfers between devices: 39.6 us -> 0.02 us  [body(): lax.psum_scatter(jnp.dot(picked, timemix_exit_weights, preferred_element_...]
    unnamed x49 -> x92, local copies, waits for them, and re-layouts: 14.9 us -> 35.6 us
    transpose x0 -> x1, local copies, waits for them, and re-layouts: none -> 15.1 us  [joined_along(): return jnp.moveaxis(blocks, 0, dim).reshape(dims)]
  transfers between devices with their start and end apart: 8 -> 22, of which waited for: 7 -> 11; matrix products, arithmetic and copies ran while one was open for 7% -> 12% of each run, Pallas kernels for 0% -> 0%
where the time goes in v1:
time: 1170 us; the launch traced here: 1150 us
  waiting for transfers between devices  319 us (27%)
  matrix products  311 us (27%)
  local copies, waits for them, and re-layouts  297 us (25%)
  starting transfers between devices  138 us (12%)
  other arithmetic  63 us (5%)
  between operations  14.4 us (1%)
    ppermute x7, starting transfers between devices, ring_gather(): upper.append(lax.ppermute(upper[-1] if upper else x, axis, back))  128 us
    ppermute x8, waiting for transfers between devices, ring_gather(): lower.append(lax.ppermute(lower[-1] if lower else x, axis, pairs))  106 us
    all_gather x1, waiting for transfers between devices, body(): lax.all_gather(widening_projection, 'sp', axis=0, tiled=True)  87.5 us
    pad x8, local copies, waits for them, and re-layouts, recurrence(): lax.associative_scan(compose, (block_maps, block_states))  86 us
    dot_general x16, matrix products, span_step(): along = jnp.einsum('bhij,bhj->bhi', state, erase_dir, precision=highest)  79.9 us
    dot_general x16, matrix products, span_step(): jnp.einsum('bhij,bhj->bhi', state, acceptor_entries, precision=highest)  79 us
    ppermute x7, waiting for transfers between devices, ring_gather(): upper.append(lax.ppermute(upper[-1] if upper else x, axis, back))  71.5 us
    dynamic_update_slice x32, local copies, waits for them, and re-layouts, recurrence(): lax.scan(span_step, (zero_state, start_maps), arranged)  57.1 us
  transfers between devices with their start and end apart: 22, of which 11 were waited for; matrix products, arithmetic and copies ran while one was open for 12% of the time, Pallas kernels for 0%

profile of v1, /device:TPU:0, one launch (start us, length us, event | category | flops | bytes accessed | tf_op | source)
XLA Modules:
  0.0 1146.0 jit_solution(7805709490829501124)
XLA Ops:
  23.2 418.4 %while.30 = (s32[]{:T(128)}, f32[8,8,64,64]{3,2,1,0:T(8,128)}, f32[8,8,64,64]{3,2,1,0:T(8,128)}, f32[16,8,8,64]{3,0,2,1:T(8,128)}, f32[16,8,8,64]{3,0,2,1:T(8,12...) while((s32[]{:T(128)}, f32[8,8,64,64]{3,2,1,0:T(8,128)}, ...), condition=%wide.region_2.3_spmd.clone, body=%wide.region_1.2_spmd.clone.sunk | while | flops 15204355 | bytes 25657612 | solution.py:147
  462.0 9.2 pad.48
  477.1 16.7 %pad.50 = f32[8,8,64,64]{3,2,1,0:T(8,128)} pad(f32[4,8,64,64]{3,2,1,0:T(8,128)} %copy-done.6, f32[]{:T(128)} %constant.70.clone.1), padding=1_0_1x0_0_0x0_0_0x0_0_0 | pad | bytes 1572868 | tf_op jit(solution)/shard_map/pad | solution.py:150
  496.0 16.7 %pad.49 = f32[8,8,64,64]{3,2,1,0:T(8,128)} pad(f32[4,8,64,64]{3,2,1,0:T(8,128)} %pad_maximum_fusion.1, f32[]{:T(128)} %constant.70.clone.1), padding=0_1_1x0_0_0x0_0_0x0_0_0 | pad | bytes 1572868 | tf_op jit(solution)/shard_map/pad | solution.py:150
  531.9 11.2 pad.114
  544.8 16.6 %pad.68 = f32[7,8,64,64]{3,2,1,0:T(8,128)} pad(f32[4,8,64,64]{3,2,1,0:T(8,128)} %pad_maximum_fusion.1, f32[]{:T(128)} %constant.70.clone.1), padding=0_0_1x0_0_0x0_0_0x0_0_0 | pad | bytes 1441796 | tf_op jit(solution)/shard_map/slice | solution.py:155
  562.4 11.1 pad.44
  575.7 11.2 pad.43
  593.5 46.1 %all-gather.5.cloned.1.call-done = bf16[16,8,64,64]{3,2,1,0:T(8,128)(2,1)} async-done(((bf16[1,8,64,64]{3,2,1,0:T(8,128)(2,1)}), bf16[16,8,64,64]{3,2,1,0:T(8,128)(2,1)}) %all-gather.5.cloned.1.call-update) | async-done | bytes 1048592 | tf_op jit(solution)/shard_map/all_gather | solution.py:38
  655.4 49.9 %collective-permute-done.1 = bf16[2816,128]{1,0:T(8,128)(2,1)S(1)} collective-permute-done((bf16[2816,128]{1,0:T(8,128)(2,1)}, bf16[2816,128]{1,0:T(8,128)(2,1)S(1)}, u32[]{:S(2)}, u32[]{:S(2)}) %collective-permute-start.1) | collective-permute-done | bytes 720928 | tf_op jit(solution)/shard_map/ppermute | solution.py:26
  711.0 29.8 %collective-permute-done.2 = bf16[2816,128]{1,0:T(8,128)(2,1)S(1)} collective-permute-done((bf16[2816,128]{1,0:T(8,128)(2,1)S(1)}, bf16[2816,128]{1,0:T(8,128)(2,1)S(1)}, u32[]{:S(2)}, u32[]{:S(2)}) %collective-permute-start.2) | collective-permute-done | bytes 720928 | tf_op jit(solution)/shard_map/ppermute | solution.py:26
  741.6 18.5 %collective-permute-start.10 = (bf16[2816,128]{1,0:T(8,128)(2,1)S(1)}, bf16[2816,128]{1,0:T(8,128)(2,1)S(1)}, u32[]{:S(2)}, u32[]{:S(2)}) collective-permute-start(bf16[2816,128]{1,0:T(8,128)(2,1)S(1)} %collective-permute-done.9), channel_id=1, source_target_pairs={{2,0},{4,2},{6,4},{8,6},{10,8},{12,10},{14,12},{16,14},{18,16},{20... | collective-permute-start | bytes 2162696 | tf_op jit(solution)/shard_map/ppermute | solution.py:28
  760.1 21.9 %collective-permute-done.3 = bf16[2816,128]{1,0:T(8,128)(2,1)S(1)} collective-permute-done((bf16[2816,128]{1,0:T(8,128)(2,1)S(1)}, bf16[2816,128]{1,0:T(8,128)(2,1)S(1)}, u32[]{:S(2)}, u32[]{:S(2)}) %collective-permute-start.3) | collective-permute-done | bytes 720928 | tf_op jit(solution)/shard_map/ppermute | solution.py:26
  784.5 20.6 %collective-permute-start.11 = (bf16[2816,128]{1,0:T(8,128)(2,1)S(1)}, bf16[2816,128]{1,0:T(8,128)(2,1)S(1)}, u32[]{:S(2)}, u32[]{:S(2)}) collective-permute-start(bf16[2816,128]{1,0:T(8,128)(2,1)S(1)} %collective-permute-done.10), channel_id=1, source_target_pairs={{2,0},{4,2},{6,4},{8,6},{10,8},{12,10},{14,12},{16,14},{18,16},{20... | collective-permute-start | bytes 2162696 | tf_op jit(solution)/shard_map/ppermute | solution.py:28
  820.5 21.3 %collective-permute-start.12 = (bf16[2816,128]{1,0:T(8,128)(2,1)S(1)}, bf16[2816,128]{1,0:T(8,128)(2,1)}, u32[]{:S(2)}, u32[]{:S(2)}) collective-permute-start(bf16[2816,128]{1,0:T(8,128)(2,1)S(1)} %collective-permute-done.11), channel_id=1, source_target_pairs={{2,0},{4,2},{6,4},{8,6},{10,8},{12,10},{14,12},{16,14},{18,16},{20... | collective-permute-start | bytes 2162696 | tf_op jit(solution)/shard_map/ppermute | solution.py:28
  841.9 31.5 %collective-permute-done.12 = bf16[2816,128]{1,0:T(8,128)(2,1)} collective-permute-done((bf16[2816,128]{1,0:T(8,128)(2,1)S(1)}, bf16[2816,128]{1,0:T(8,128)(2,1)}, u32[]{:S(2)}, u32[]{:S(2)}) %collective-permute-start.12) | collective-permute-done | bytes 720928 | tf_op jit(solution)/shard_map/ppermute | solution.py:28
  873.5 17.4 %collective-permute-start.13 = (bf16[2816,128]{1,0:T(8,128)(2,1)}, bf16[2816,128]{1,0:T(8,128)(2,1)}, u32[]{:S(2)}, u32[]{:S(2)}) collective-permute-start(bf16[2816,128]{1,0:T(8,128)(2,1)} %collective-permute-done.12), channel_id=1, source_target_pairs={{2,0},{4,2},{6,4},{8,6},{10,8},{12,10},{14,12},{16,14},{18,16},{20... | collective-permute-start | bytes 2162696 | tf_op jit(solution)/shard_map/ppermute | solution.py:28
  893.4 23.0 %collective-permute-done.13 = bf16[2816,128]{1,0:T(8,128)(2,1)} collective-permute-done((bf16[2816,128]{1,0:T(8,128)(2,1)}, bf16[2816,128]{1,0:T(8,128)(2,1)}, u32[]{:S(2)}, u32[]{:S(2)}) %collective-permute-start.13) | collective-permute-done | bytes 720928 | tf_op jit(solution)/shard_map/ppermute | solution.py:28
  916.5 24.0 %collective-permute-start.14 = (bf16[2816,128]{1,0:T(8,128)(2,1)}, bf16[2816,128]{1,0:T(8,128)(2,1)}, u32[]{:S(2)}, u32[]{:S(2)}) collective-permute-start(bf16[2816,128]{1,0:T(8,128)(2,1)} %collective-permute-done.13), channel_id=1, source_target_pairs={{2,0},{4,2},{6,4},{8,6},{10,8},{12,10},{14,12},{16,14},{18,16},{20... | collective-permute-start | bytes 2162696 | tf_op jit(solution)/shard_map/ppermute | solution.py:28
  951.9 20.6 %collective-permute-start.15 = (bf16[2816,128]{1,0:T(8,128)(2,1)}, bf16[2816,128]{1,0:T(8,128)(2,1)}, u32[]{:S(2)}, u32[]{:S(2)}) collective-permute-start(bf16[2816,128]{1,0:T(8,128)(2,1)} %collective-permute-done.14), channel_id=1, source_target_pairs={{2,0},{4,2},{6,4},{8,6},{10,8},{12,10},{14,12},{16,14},{18,16},{20... | collective-permute-start | bytes 2162696 | tf_op jit(solution)/shard_map/ppermute | solution.py:28
  1001.7 10.3 gather_fusion
  1012.0 15.1 %copy.92 = bf16[2816,16,128]{0,2,1:T(8,128)(2,1)} copy(bf16[2816,16,128]{2,0,1:T(8,128)(2,1)} %bitcast.222) | data formatting | bytes 23068672 | tf_op jit(solution)/shard_map/transpose | solution.py:16
  1028.5 87.5 %all-gather.11.cloned.1.call-done = bf16[2048,2816]{1,0:T(8,128)(2,1)} async-done(((bf16[128,2816]{1,0:T(8,128)(2,1)}), bf16[2048,2816]{1,0:T(8,128)(2,1)}) %all-gather.11.cloned.1.call-update) | async-done | bytes 11534352 | tf_op jit(solution)/shard_map/all_gather | solution.py:180
  1116.0 14.9 %convolution_convert_fusion.2 = bf16[128,2048]{1,0:T(8,128)(2,1)} fusion(bf16[2816,2048]{0,1:T(8,128)(2,1)} %bitcast.223, bf16[128,2048]{1,0:T(8,128)(2,1)S(1)} %all_gather.19, bf16[2048,2816]{1,0:T(8,128)(2,1)} %all-gather.11.cloned.1.call-done, f32[130,2816]{1,0:T(8,128)} %maximum_convert_fusion, f32[2816]{0:T(1024)S(1)} %get-tuple-element.204, ...), kind=kOutput, calls=%fused_computation.28 | convolution fusion | flops 2957737984 | bytes 28476416 | tf_op jit(solution)/shard_map/dot_general | solution.py:227
  (500 shorter events, 585.5 us)
Async XLA Ops:
  6.5 642.3 %copy-start = (bf16[512,2048]{1,0:T(8,128)(2,1)S(1)}, bf16[512,2048]{1,0:T(8,128)(2,1)}, u32[]{:S(2)}) copy-start(bf16[512,2048]{1,0:T(8,128)(2,1)} %param.27) | copy-start | bytes 6291460
  6.5 587.0 %all-gather.7.cloned.1.call-start = ((), (), s32[]{:S(2)}) async-start(), calls=%async_computation.3 | async-start | bytes 2228224 | tf_op jit(solution)/shard_map/all_gather | solution.py:38
  514.4 125.2 %all-gather.5.cloned.1.call-start = ((), (), s32[]{:S(2)}) async-start(), calls=%async_computation.2 | async-start | bytes 2228224 | tf_op jit(solution)/shard_map/all_gather | solution.py:38
  544.8 347.5 %reduce-scatter.3.cloned.1.call-start = ((), (), s32[]{:S(2)}) async-start(), calls=%async_computation.4 | async-start | bytes 786432 | tf_op jit(solution)/shard_map/reduce_scatter | solution.py:198
  651.1 289.3 %copy-start.38 = (f32[2048]{0:T(1024)S(1)}, f32[2048]{0:T(1024)}, u32[]{:S(2)}) copy-start(f32[2048]{0:T(1024)} %param.29) | copy-start | bytes 24580
  651.1 341.0 %all-gather.9.cloned.1.call-start = ((), (), s32[]{:S(2)}) async-start(), calls=%async_computation.5 | async-start | bytes 12255232 | tf_op jit(solution)/shard_map/all_gather | solution.py:179
  651.7 464.3 %all-gather.11.cloned.1.call-start = ((), (), s32[]{:S(2)}) async-start(), calls=%async_computation.6 | async-start | bytes 12255232 | tf_op jit(solution)/shard_map/all_gather | solution.py:180
  652.3 484.9 %reduce-scatter.5.cloned.1.call-start = ((), (), s32[]{:S(2)}) async-start(), calls=%async_computation.7 | async-start | bytes 786432 | tf_op jit(solution)/shard_map/reduce_scatter | solution.py:226
  652.3 53.0 %collective-permute-start.1 = (bf16[2816,128]{1,0:T(8,128)(2,1)}, bf16[2816,128]{1,0:T(8,128)(2,1)S(1)}, u32[]{:S(2)}, u32[]{:S(2)}) collective-permute-start(bf16[2816,128]{1,0:T(8,128)(2,1)} %param.33), channel_id=1, source_target_pairs={{0,2},{2,4},{4,6},{6,8},{8,10},{10,12},{12,14},{14,16},{16,18},{18... | collective-permute-start | bytes 2162696 | tf_op jit(solution)/shard_map/ppermute | solution.py:26
  705.3 35.4 %collective-permute-start.2 = (bf16[2816,128]{1,0:T(8,128)(2,1)S(1)}, bf16[2816,128]{1,0:T(8,128)(2,1)S(1)}, u32[]{:S(2)}, u32[]{:S(2)}) collective-permute-start(bf16[2816,128]{1,0:T(8,128)(2,1)S(1)} %collective-permute-done.1), channel_id=1, source_target_pairs={{0,2},{2,4},{4,6},{6,8},{8,10},{10,12},{12,14},{14,16},{16,18},{18... | collective-permute-start | bytes 2162696 | tf_op jit(solution)/shard_map/ppermute | solution.py:26
  705.3 35.4 %collective-permute-start.9 = (bf16[2816,128]{1,0:T(8,128)(2,1)}, bf16[2816,128]{1,0:T(8,128)(2,1)S(1)}, u32[]{:S(2)}, u32[]{:S(2)}) collective-permute-start(bf16[2816,128]{1,0:T(8,128)(2,1)} %param.33), channel_id=1, source_target_pairs={{2,0},{4,2},{6,4},{8,6},{10,8},{12,10},{14,12},{16,14},{18,16},{20... | collective-permute-start | bytes 2162696 | tf_op jit(solution)/shard_map/ppermute | solution.py:28
  740.7 41.3 %collective-permute-start.3 = (bf16[2816,128]{1,0:T(8,128)(2,1)S(1)}, bf16[2816,128]{1,0:T(8,128)(2,1)S(1)}, u32[]{:S(2)}, u32[]{:S(2)}) collective-permute-start(bf16[2816,128]{1,0:T(8,128)(2,1)S(1)} %collective-permute-done.2), channel_id=1, source_target_pairs={{0,2},{2,4},{4,6},{6,8},{8,10},{10,12},{12,14},{14,16},{16,18},{18... | collective-permute-start | bytes 2162696 | tf_op jit(solution)/shard_map/ppermute | solution.py:26
  741.6 42.9 %collective-permute-start.10 = (bf16[2816,128]{1,0:T(8,128)(2,1)S(1)}, bf16[2816,128]{1,0:T(8,128)(2,1)S(1)}, u32[]{:S(2)}, u32[]{:S(2)}) collective-permute-start(bf16[2816,128]{1,0:T(8,128)(2,1)S(1)} %collective-permute-done.9), channel_id=1, source_target_pairs={{2,0},{4,2},{6,4},{8,6},{10,8},{12,10},{14,12},{16,14},{18,16},{20... | collective-permute-start | bytes 2162696 | tf_op jit(solution)/shard_map/ppermute | solution.py:28
  782.0 27.7 %collective-permute-start.4 = (bf16[2816,128]{1,0:T(8,128)(2,1)S(1)}, bf16[2816,128]{1,0:T(8,128)(2,1)S(1)}, u32[]{:S(2)}, u32[]{:S(2)}) collective-permute-start(bf16[2816,128]{1,0:T(8,128)(2,1)S(1)} %collective-permute-done.3), channel_id=1, source_target_pairs={{0,2},{2,4},{4,6},{6,8},{8,10},{10,12},{12,14},{14,16},{16,18},{18... | collective-permute-start | bytes 2162696 | tf_op jit(solution)/shard_map/ppermute | solution.py:26
  784.5 36.0 %collective-permute-start.11 = (bf16[2816,128]{1,0:T(8,128)(2,1)S(1)}, bf16[2816,128]{1,0:T(8,128)(2,1)S(1)}, u32[]{:S(2)}, u32[]{:S(2)}) collective-permute-start(bf16[2816,128]{1,0:T(8,128)(2,1)S(1)} %collective-permute-done.10), channel_id=1, source_target_pairs={{2,0},{4,2},{6,4},{8,6},{10,8},{12,10},{14,12},{16,14},{18,16},{20... | collective-permute-start | bytes 2162696 | tf_op jit(solution)/shard_map/ppermute | solution.py:28
  809.8 32.1 %collective-permute-start.5 = (bf16[2816,128]{1,0:T(8,128)(2,1)S(1)}, bf16[2816,128]{1,0:T(8,128)(2,1)S(1)}, u32[]{:S(2)}, u32[]{:S(2)}) collective-permute-start(bf16[2816,128]{1,0:T(8,128)(2,1)S(1)} %collective-permute-done.4), channel_id=1, source_target_pairs={{0,2},{2,4},{4,6},{6,8},{8,10},{10,12},{12,14},{14,16},{16,18},{18... | collective-permute-start | bytes 2162696 | tf_op jit(solution)/shard_map/ppermute | solution.py:26
  820.5 53.0 %collective-permute-start.12 = (bf16[2816,128]{1,0:T(8,128)(2,1)S(1)}, bf16[2816,128]{1,0:T(8,128)(2,1)}, u32[]{:S(2)}, u32[]{:S(2)}) collective-permute-start(bf16[2816,128]{1,0:T(8,128)(2,1)S(1)} %collective-permute-done.11), channel_id=1, source_target_pairs={{2,0},{4,2},{6,4},{8,6},{10,8},{12,10},{14,12},{16,14},{18,16},{20... | collective-permute-start | bytes 2162696 | tf_op jit(solution)/shard_map/ppermute | solution.py:28
  841.8 49.0 %collective-permute-start.6 = (bf16[2816,128]{1,0:T(8,128)(2,1)S(1)}, bf16[2816,128]{1,0:T(8,128)(2,1)}, u32[]{:S(2)}, u32[]{:S(2)}) collective-permute-start(bf16[2816,128]{1,0:T(8,128)(2,1)S(1)} %collective-permute-done.5), channel_id=1, source_target_pairs={{0,2},{2,4},{4,6},{6,8},{8,10},{10,12},{12,14},{14,16},{16,18},{18... | collective-permute-start | bytes 2162696 | tf_op jit(solution)/shard_map/ppermute | solution.py:26
  873.5 43.0 %collective-permute-start.13 = (bf16[2816,128]{1,0:T(8,128)(2,1)}, bf16[2816,128]{1,0:T(8,128)(2,1)}, u32[]{:S(2)}, u32[]{:S(2)}) collective-permute-start(bf16[2816,128]{1,0:T(8,128)(2,1)} %collective-permute-done.12), channel_id=1, source_target_pairs={{2,0},{4,2},{6,4},{8,6},{10,8},{12,10},{14,12},{16,14},{18,16},{20... | collective-permute-start | bytes 2162696 | tf_op jit(solution)/shard_map/ppermute | solution.py:28
  890.9 49.6 %collective-permute-start.7 = (bf16[2816,128]{1,0:T(8,128)(2,1)}, bf16[2816,128]{1,0:T(8,128)(2,1)}, u32[]{:S(2)}, u32[]{:S(2)}) collective-permute-start(bf16[2816,128]{1,0:T(8,128)(2,1)} %collective-permute-done.6), channel_id=1, source_target_pairs={{0,2},{2,4},{4,6},{6,8},{8,10},{10,12},{12,14},{14,16},{16,18},{18... | collective-permute-start | bytes 2162696 | tf_op jit(solution)/shard_map/ppermute | solution.py:26
  916.5 35.4 %collective-permute-start.14 = (bf16[2816,128]{1,0:T(8,128)(2,1)}, bf16[2816,128]{1,0:T(8,128)(2,1)}, u32[]{:S(2)}, u32[]{:S(2)}) collective-permute-start(bf16[2816,128]{1,0:T(8,128)(2,1)} %collective-permute-done.13), channel_id=1, source_target_pairs={{2,0},{4,2},{6,4},{8,6},{10,8},{12,10},{14,12},{16,14},{18,16},{20... | collective-permute-start | bytes 2162696 | tf_op jit(solution)/shard_map/ppermute | solution.py:28
  940.4 32.0 %collective-permute-start.8 = (bf16[2816,128]{1,0:T(8,128)(2,1)}, bf16[2816,128]{1,0:T(8,128)(2,1)S(1)}, u32[]{:S(2)}, u32[]{:S(2)}) collective-permute-start(bf16[2816,128]{1,0:T(8,128)(2,1)} %collective-permute-done.7), channel_id=1, source_target_pairs={{0,2},{2,4},{4,6},{6,8},{8,10},{10,12},{12,14},{14,16},{16,18},{18... | collective-permute-start | bytes 2162696 | tf_op jit(solution)/shard_map/ppermute | solution.py:26
  951.9 47.8 %collective-permute-start.15 = (bf16[2816,128]{1,0:T(8,128)(2,1)}, bf16[2816,128]{1,0:T(8,128)(2,1)}, u32[]{:S(2)}, u32[]{:S(2)}) collective-permute-start(bf16[2816,128]{1,0:T(8,128)(2,1)} %collective-permute-done.14), channel_id=1, source_target_pairs={{2,0},{4,2},{6,4},{8,6},{10,8},{12,10},{14,12},{16,14},{18,16},{20... | collective-permute-start | bytes 2162696 | tf_op jit(solution)/shard_map/ppermute | solution.py:28
  998.2 29.0 %collective-permute-start = (bf16[2,2816]{1,0:T(2,128)(2,1)S(1)}, bf16[2,2816]{1,0:T(2,128)(2,1)S(1)}, u32[]{:S(2)}, u32[]{:S(2)}) collective-permute-start(bf16[2,2816]{1,0:T(2,128)(2,1)S(1)} %slice.168), channel_id=1, source_target_pairs={{0,2},{2,4},{4,6},{6,8},{8,10},{10,12},{12,14},{14,16},{16,18},{18... | collective-permute-start | bytes 33800 | tf_op jit(solution)/shard_map/ppermute | solution.py:58
  (99 other events, 1009.9 us)
Sparse Core Ops, SparseCore 0:
  514.5 63.0 all-gather.6
  580.4 59.1 all-gather.4
  651.2 41.1 reduce-scatter.2
  695.1 254.1 all-gather.8
  951.9 164.0 all-gather.10
  1131.0 6.0 reduce-scatter.4
